TPU v7x, 32 devices: a whole 2x2x4 slice. The times are simulated.
32 devices in a mesh: fs: 16 (over z, y, x), tp: 2 (over core).
Axes of the slice: x: 2, y: 2, z: 4, core: 2. Of those that a mesh axis runs over, the one named last changes fastest.
Arguments:
- saved_inputs: bfloat16 [2048, 4096], P('fs', 'tp'), may hold values from -6 to 6
- value_cotangent: bfloat16 [2048, 2048], P('fs'), may hold values from -0.1875 to 0.1875
- glu_output: bfloat16 [2048, 2048], P('fs', 'tp'), may hold values from -6 to 6
- conv_cotangent: bfloat16 [2048, 2048], P('fs', 'tp'), may hold values from -0.125 to 0.125
- factor: bfloat16 [4096, 256], P('tp'), may hold values from -0.09375 to 0.09375
- value_weight: float32 [2048, 4096], P('fs', 'tp'), may hold values from -3 to 3
- first_moment: float32 [2048, 256], P('fs', 'tp'), may hold values from -6 to 6
- second_moment: float32 [2048, 256], P('fs', 'tp'), may hold values from 0.25 to 4
- kernel: float32 [31, 2048], P(None, 'tp'), may hold values from -1 to 1
- kernel_first: float32 [31, 2048], P(None, 'tp'), may hold values from -6 to 6
- kernel_second: float32 [31, 2048], P(None, 'tp'), may hold values from 0.25 to 4
Outputs:
- new_value: float32 [2048, 4096], P('fs', 'tp')
- value_copy: bfloat16 [2048, 4096], P('fs', 'tp')
- value_step: float32 [2048, 4096], P('fs', 'tp')
- new_first: float32 [2048, 256], P('fs', 'tp')
- new_second: float32 [2048, 256], P('fs', 'tp')
- new_kernel: float32 [31, 2048], P(None, 'tp')
- new_kernel_first: float32 [31, 2048], P(None, 'tp')
- new_kernel_second: float32 [31, 2048], P(None, 'tp')
All inputs are finite; a program needn't handle non-finite values.
Results may differ from a plain program's by a relative error of at most 0.0055.
Values may be sent and summed in bfloat16 or wider, within the bound.
A program may use at most 64 MiB of HBM per device.

v0:
```python
import jax
import jax.numpy as jnp
from jax import lax
from jax.sharding import PartitionSpec as P

WIDTH = 4096


def from_behind(x, axis, by):
    peers = lax.axis_size(axis)
    pairs = [(i, i + by) for i in range(peers) if 0 <= i + by < peers]
    return lax.ppermute(x, axis, pairs)


def body(
    saved_inputs,
    value_cotangent,
    glu_output,
    conv_cotangent,
    factor,
    value_weight,
    first_moment,
    second_moment,
    kernel,
    kernel_first,
    kernel_second,
):
    highest = lax.Precision.HIGHEST
    factor_f = factor.astype(jnp.float32)
    partial_reduced = jnp.dot(saved_inputs, factor, preferred_element_type=jnp.float32)
    reduced = lax.psum_scatter(
        partial_reduced.astype(jnp.bfloat16), "tp", scatter_dimension=1, tiled=True
    ).astype(jnp.float32)
    upper_part = reduced.astype(jnp.bfloat16)
    lower_part = (reduced - upper_part.astype(jnp.float32)).astype(jnp.bfloat16)
    dims = (((0,), (0,)), ((), ()))
    upper_term = lax.dot_general(
        value_cotangent, upper_part, dims, preferred_element_type=jnp.float32
    )
    lower_term = lax.dot_general(
        value_cotangent, lower_part, dims, preferred_element_type=jnp.float32
    )
    projected = lax.psum_scatter(upper_term + lower_term, "fs", scatter_dimension=0, tiled=True)
    new_first = 0.8 * first_moment + 0.2 * projected
    new_second = 0.9 * second_moment + 0.1 * projected * projected
    direction = new_first / jnp.sqrt(new_second)
    full_direction = lax.all_gather(direction, "tp", axis=1, tiled=True)
    back_proj = jnp.dot(full_direction, factor_f.T, precision=highest)
    row_squares = lax.psum(jnp.sum(back_proj * back_proj, axis=1), "tp")
    value_step = back_proj / jnp.sqrt(row_squares / WIDTH + 0.01)[:, None]
    new_value = value_weight - 0.05 * value_step
    value_copy = new_value.astype(jnp.bfloat16)
    token_count = glu_output.shape[0]
    reach = kernel.shape[0] - 1
    halo_rows = from_behind(glu_output[token_count - reach :], "fs", 1)
    extended = jnp.concatenate([halo_rows, glu_output], axis=0).astype(jnp.float32)
    cotangent_f = conv_cotangent.astype(jnp.float32)
    pieces = []
    for offset in range(kernel.shape[0]):
        begin = reach - offset
        pieces.append(jnp.sum(extended[begin : begin + token_count] * cotangent_f, axis=0))
    local_grad = jnp.stack(pieces, axis=0)
    kernel_grad = lax.psum(local_grad, "fs")
    new_kernel_first = 0.8 * kernel_first + 0.2 * kernel_grad
    new_kernel_second = 0.9 * kernel_second + 0.1 * kernel_grad * kernel_grad
    new_kernel = kernel - 0.05 * new_kernel_first / jnp.sqrt(new_kernel_second)
    return (
        new_value,
        value_copy,
        value_step,
        new_first,
        new_second,
        new_kernel,
        new_kernel_first,
        new_kernel_second,
    )


def solution(mesh):
    placed = (
        P("fs", "tp"),
        P("fs", None),
        P("fs", "tp"),
        P("fs", "tp"),
        P("tp", None),
        P("fs", "tp"),
        P("fs", "tp"),
        P("fs", "tp"),
        P(None, "tp"),
        P(None, "tp"),
        P(None, "tp"),
    )
    return jax.shard_map(
        body,
        mesh=mesh,
        in_specs=placed,
        out_specs=(
            P("fs", "tp"),
            P("fs", "tp"),
            P("fs", "tp"),
            P("fs", "tp"),
            P("fs", "tp"),
            P(None, "tp"),
            P(None, "tp"),
            P(None, "tp"),
        ),
        check_vma=False,
    )
```

profile of v0, /device:TPU:0, one launch (start us, length us, event | category | flops | bytes accessed | tf_op | source)
XLA Modules:
  0.0 225.3 jit_solution(7543839092658024599)
XLA Ops:
  8.0 0.0 reduce-scatter.7.cloned.1.call-start
  8.1 0.9 slice.96
  9.0 4.9 %collective-permute-start = (bf16[30,1024]{1,0:T(8,128)(2,1)S(1)}, bf16[30,1024]{1,0:T(8,128)(2,1)S(1)}, u32[]{:S(2)}, u32[]{:S(2)}) collective-permute-start(bf16[30,1024]{1,0:T(8,128)(2,1)S(1)} %slice.96), channel_id=1, source_target_pairs={{0,2},{2,4},{4,6},{6,8},{8,10},{10,12},{12,14},{14,16},{16,18},{18... | collective-permute-start | bytes 184328 | tf_op jit(solution)/shard_map/ppermute | solution.py:12
  13.9 1.4 convolution_convert_fusion
  15.3 0.7 copy.27
  16.0 0.0 reduce-scatter.7.cloned.1.call-update
  16.1 0.0 all-reduce.2.cloned.1.call-start
  16.1 0.1 maximum_convert_fusion
  16.2 0.8 copy-done.3
  17.0 1.1 fusion.31
  18.1 0.8 fusion.30
  18.9 2.7 %stack.127 = f32[31,1024]{1,0:T(8,128)} concatenate(f32[1,1024]{1,0:T(1,128)S(1)} %bitcast.75, f32[1,1024]{1,0:T(1,128)S(1)} %bitcast.46, f32[1,1024]{1,0:T(1,128)S(1)} %bitcast.47, f32[1,1024]{1,0:T(1,128)S(1)} %bitcast.48, f32[1,1024]{1,0:T(1,128)S(1)} %bitcast.49, f32[1,1024]{1,0:T(1,128)S(1)} %bitcast.50, f32[1,1024]{1,0:T(1,128)S(1)} %bitcast.51, f32[1,1024]{1,0:T(1,128)S(1)} %bitcast.52, ...), dimensions={0} | concatenate | bytes 253952 | tf_op jit(solution)/shard_map/stack | solution.py:62
  21.6 0.0 all-reduce.2.cloned.1.call-update
  21.6 0.0 reduce-scatter.5.cloned.1.call-start
  21.7 2.4 %reduce-scatter.7.cloned.1.call-done = bf16[128,128]{1,0:T(8,128)(2,1)} async-done(((bf16[256,128]{1,0:T(8,128)(2,1)}), bf16[128,128]{1,0:T(8,128)(2,1)}) %reduce-scatter.7.cloned.1.call-update) | async-done | bytes 32784
  24.1 0.9 copy.28
  25.0 0.3 fusion.34
  25.3 1.3 fusion
  26.6 0.0 reduce-scatter.5.cloned.1.call-update
  26.6 0.8 copy-done.9
  27.5 0.1 copy.24
  27.6 0.1 copy.23
  27.7 100.1 %all-reduce.2.cloned.1.call-done = f32[31,1024]{1,0:T(8,128)} async-done(((f32[31,1024]{1,0:T(8,128)}), f32[31,1024]{1,0:T(8,128)}) %all-reduce.2.cloned.1.call-update) | async-done | bytes 126992 | tf_op jit(solution)/shard_map/psum | solution.py:63
  127.7 1.7 multiply_subtract_fusion.1
  129.4 78.8 %reduce-scatter.5.cloned.1.call-done = f32[128,128]{0,1:T(8,128)} async-done(((f32[2048,128]{0,1:T(8,128)}), f32[128,128]{0,1:T(8,128)}) %reduce-scatter.5.cloned.1.call-update) | async-done | bytes 65552 | tf_op jit(solution)/shard_map/reduce_scatter | solution.py:43
  208.2 0.9 rsqrt_multiply_fusion
  209.1 1.9 all_gather.3
  211.0 1.1 multiply_reduce_fusion
  212.1 2.5 %psum.14 = f32[128]{0:T(128)S(1)} all-reduce(f32[128]{0:T(128)S(1)} %get-tuple-element.64), channel_id=1, replica_groups=mesh['fs'=16,'tp'=2] {'tp'}, use_global_device_ids=true, to_apply=%region_3.0 | all-reduce | flops 128 | bytes 1024 | tf_op jit(solution)/shard_map/psum | solution.py:49
  214.5 0.7 copy.25
  215.3 0.7 copy.26
  216.0 1.8 fusion.37
  (22 shorter events, 0.1 us)
Async XLA Ops:
  8.0 5.9 %copy-start = (bf16[2048,256]{1,0:T(8,128)(2,1)S(1)}, bf16[2048,256]{1,0:T(8,128)(2,1)}, u32[]{:S(2)}) copy-start(bf16[2048,256]{1,0:T(8,128)(2,1)} %param.15) | copy-start | bytes 3145732
  8.0 16.1 %reduce-scatter.7.cloned.1.call-start = ((), (), s32[]{:S(2)}) async-start(), calls=%async_computation.4 | async-start | bytes 98304
  9.0 7.1 %collective-permute-start = (bf16[30,1024]{1,0:T(8,128)(2,1)S(1)}, bf16[30,1024]{1,0:T(8,128)(2,1)S(1)}, u32[]{:S(2)}, u32[]{:S(2)}) collective-permute-start(bf16[30,1024]{1,0:T(8,128)(2,1)S(1)} %slice.96), channel_id=1, source_target_pairs={{0,2},{2,4},{4,6},{6,8},{8,10},{10,12},{12,14},{14,16},{16,18},{18... | collective-permute-start | bytes 184328 | tf_op jit(solution)/shard_map/ppermute | solution.py:12
  13.9 2.2 copy-start.4
  16.1 1.0 copy-start.3
  16.1 111.7 %all-reduce.2.cloned.1.call-start = ((), (), s32[]{:S(2)}) async-start(), calls=%async_computation.3 | async-start | bytes 262144 | tf_op jit(solution)/shard_map/psum | solution.py:63
  18.9 6.1 %copy-start.1 = (bf16[128,2048]{1,0:T(8,128)(2,1)S(1)}, bf16[128,2048]{1,0:T(8,128)(2,1)}, u32[]{:S(2)}) copy-start(bf16[128,2048]{1,0:T(8,128)(2,1)} %param.12) | copy-start | bytes 1572868
  21.6 186.6 %reduce-scatter.5.cloned.1.call-start = ((), (), s32[]{:S(2)}) async-start(), calls=%async_computation.2 | async-start | bytes 1114112 | tf_op jit(solution)/shard_map/reduce_scatter | solution.py:43
  24.1 1.0 copy-start.8
  26.6 0.8 copy-start.9
  26.6 0.9 copy-start.10
  26.6 101.1 %copy-start.7 = (f32[31,1024]{1,0:T(8,128)S(1)}, f32[31,1024]{1,0:T(8,128)}, u32[]{:S(2)}) copy-start(f32[31,1024]{1,0:T(8,128)} %param.21) | copy-start | bytes 380932
  27.5 100.3 %copy-start.5 = (f32[31,1024]{1,0:T(8,128)S(1)}, f32[31,1024]{1,0:T(8,128)}, u32[]{:S(2)}) copy-start(f32[31,1024]{1,0:T(8,128)} %param.19) | copy-start | bytes 380932
  27.5 100.3 %copy-start.6 = (f32[31,1024]{1,0:T(8,128)S(1)}, f32[31,1024]{1,0:T(8,128)}, u32[]{:S(2)}) copy-start(f32[31,1024]{1,0:T(8,128)} %param.20) | copy-start | bytes 380932
  211.0 5.0 %copy-start.2 = (f32[128,2048]{1,0:T(8,128)S(1)}, f32[128,2048]{1,0:T(8,128)}, u32[]{:S(2)}) copy-start(f32[128,2048]{1,0:T(8,128)} %param.16) | copy-start | bytes 3145732
Sparse Core Ops, SparseCore 0:
  16.2 7.8 reduce-scatter.6
Sparse Core Ops, SparseCore 1:
  22.6 105.1 all-reduce.1
  130.4 77.7 reduce-scatter.4
where the time goes:
time: 226 us; the launch traced here: 225 us
  waiting for transfers between devices  181 us (80%)
  between operations  15.6 us (7%)
  local copies, waits for them, and re-layouts  8.54 us (4%)
  other arithmetic  6.33 us (3%)
  starting transfers between devices  5 us (2%)
  blocking collectives  4.37 us (2%)
  matrix products  4.05 us (2%)
    psum x1, waiting for transfers between devices, body(): kernel_grad = lax.psum(local_grad, 'fs')  100 us
    reduce_scatter x1, waiting for transfers between devices, body(): lax.psum_scatter(upper_term + lower_term, 'fs', scatter_dimension=0, tile...  78.8 us
    unnamed x28, local copies, waits for them, and re-layouts  4.95 us
    ppermute x1, starting transfers between devices, from_behind(): return lax.ppermute(x, axis, pairs)  4.87 us
  transfers between devices with their start and end apart: 4, of which 3 were waited for; matrix products, arithmetic and copies ran while one was open for 5% of the time, Pallas kernels for 0%

commit v1 on v0

--- a/solution.py
+++ b/solution.py
@@ -4,6 +4,17 @@
 from jax.sharding import PartitionSpec as P
 
 WIDTH = 4096
+
+
+def fill_cubes_now(tile_in):
+    along_axis = "fs"
+    n = lax.axis_size(along_axis)
+    view_out = tile_in
+    for tick in [to_i for to_i in (1, 2, 4, 8, 16) if to_i < n]:
+        view_out = view_out + lax.ppermute(
+            view_out, axis_name=along_axis, perm=list(map(lambda t: (t, t ^ tick), range(n)))
+        )
+    return view_out
 
 
 def from_behind(x, axis, by):
@@ -60,7 +71,7 @@
         begin = reach - offset
         pieces.append(jnp.sum(extended[begin : begin + token_count] * cotangent_f, axis=0))
     local_grad = jnp.stack(pieces, axis=0)
-    kernel_grad = lax.psum(local_grad, "fs")
+    kernel_grad = fill_cubes_now(local_grad)
     new_kernel_first = 0.8 * kernel_first + 0.2 * kernel_grad
     new_kernel_second = 0.9 * kernel_second + 0.1 * kernel_grad * kernel_grad
     new_kernel = kernel - 0.05 * new_kernel_first / jnp.sqrt(new_kernel_second)

time: 226 us -> 121 us (0.54)
  waiting for transfers between devices: 181 us -> 70.4 us
  starting transfers between devices: 5 us -> 16.3 us
  local copies, waits for them, and re-layouts: 8.54 us -> 5.71 us
    psum x1 -> x0, waiting for transfers between devices: 100 us -> none  [body(): kernel_grad = lax.psum(local_grad, 'fs')]
    reduce_scatter x1, waiting for transfers between devices: 78.8 us -> 42.4 us  [body(): lax.psum_scatter(upper_term + lower_term, 'fs', scatter_dimension=0, tile...]
    ppermute x0 -> x4, waiting for transfers between devices: none -> 15.6 us  [fill_cubes_now(): lax.ppermute(view_out, axis_name=along_axis, perm=list(map(lambda t: (t,...]
    ppermute x0 -> x4, starting transfers between devices: none -> 12.5 us  [fill_cubes_now(): lax.ppermute(view_out, axis_name=along_axis, perm=list(map(lambda t: (t,...]
    unnamed x4 -> x3, waiting for transfers between devices: 2.46 us -> 10.5 us
    another operation x1, local copies, waits for them, and re-layouts: 2.66 us -> 0.24 us  [body(): local_grad = jnp.stack(pieces, axis=0)]
  transfers between devices with their start and end apart: 4 -> 7, of which waited for: 3 -> 7; matrix products, arithmetic and copies ran while one was open for 5% -> 3% of each run, Pallas kernels for 0% -> 0%
where the time goes in v1:
time: 121 us; the launch traced here: 120 us
  waiting for transfers between devices  70.4 us (58%)
  starting transfers between devices  16.3 us (13%)
  between operations  14.2 us (12%)
  local copies, waits for them, and re-layouts  5.71 us (5%)
  other arithmetic  5.49 us (5%)
  blocking collectives  4.37 us (4%)
  matrix products  4.06 us (3%)
    reduce_scatter x1, waiting for transfers between devices, body(): lax.psum_scatter(upper_term + lower_term, 'fs', scatter_dimension=0, tile...  42.4 us
    ppermute x4, waiting for transfers between devices, fill_cubes_now(): lax.ppermute(view_out, axis_name=along_axis, perm=list(map(lambda t: (t,...  15.6 us
    ppermute x4, starting transfers between devices, fill_cubes_now(): lax.ppermute(view_out, axis_name=along_axis, perm=list(map(lambda t: (t,...  12.5 us
    unnamed x3, waiting for transfers between devices  10.5 us
    unnamed x28, local copies, waits for them, and re-layouts  5.45 us
    ppermute x1, starting transfers between devices, from_behind(): return lax.ppermute(x, axis, pairs)  3.72 us
    psum x1, blocking collectives, body(): row_squares = lax.psum(jnp.sum(back_proj * back_proj, axis=1), 'tp')  2.47 us
  transfers between devices with their start and end apart: 7, of which 7 were waited for; matrix products, arithmetic and copies ran while one was open for 3% of the time, Pallas kernels for 0%

profile of v1, /device:TPU:0, one launch (start us, length us, event | category | flops | bytes accessed | tf_op | source)
XLA Modules:
  0.0 120.5 jit_solution(5931972066683388435)
XLA Ops:
  7.2 1.2 copy-done
  8.4 1.4 %convolution_convert_fusion = bf16[128,256]{1,0:T(8,128)(2,1)S(1)} fusion(bf16[128,2048]{1,0:T(8,128)(2,1)} %param.11, bf16[2048,256]{1,0:T(8,128)(2,1)S(1)} %copy-done), kind=kOutput, calls=%fused_computation.33 | convolution fusion | flops 134250496 | bytes 1638400 | tf_op jit(solution)/shard_map/dot_general | solution.py:41
  9.8 0.7 copy.27
  10.6 10.4 %reduce-scatter.7.cloned.1.call-done = bf16[128,128]{1,0:T(8,128)(2,1)} async-done(((bf16[256,128]{1,0:T(8,128)(2,1)}), bf16[128,128]{1,0:T(8,128)(2,1)}) %reduce-scatter.7.cloned.1.call-update) | async-done | bytes 32784
  21.0 0.9 copy.28
  22.0 0.3 fusion.34
  22.3 1.3 %fusion = f32[2048,128]{0,1:T(8,128)} fusion(f32[128,2048]{1,0:T(8,128)S(1)} %fusion.34, bf16[128,2048]{1,0:T(8,128)(2,1)S(1)} %copy-done.1, bf16[128,128]{1,0:T(8,128)(2,1)S(1)} %copy.28), kind=kOutput, calls=%fused_computation.32 | convolution fusion | flops 67420160 | bytes 2654208 | tf_op jit(solution)/shard_map/dot_general | solution.py:51
  23.6 0.9 copy-done.4
  24.6 3.7 %collective-permute-start = (bf16[30,1024]{1,0:T(8,128)(2,1)S(1)}, bf16[30,1024]{1,0:T(8,128)(2,1)S(1)}, u32[]{:S(2)}, u32[]{:S(2)}) collective-permute-start(bf16[30,1024]{1,0:T(8,128)(2,1)S(1)} %slice.96), channel_id=1, source_target_pairs={{0,2},{2,4},{4,6},{6,8},{8,10},{10,12},{12,14},{14,16},{16,18},{18... | collective-permute-start | bytes 184328 | tf_op jit(solution)/shard_map/ppermute | solution.py:23
  28.3 1.9 %collective-permute-done = bf16[30,1024]{1,0:T(8,128)(2,1)S(1)} collective-permute-done((bf16[30,1024]{1,0:T(8,128)(2,1)S(1)}, bf16[30,1024]{1,0:T(8,128)(2,1)S(1)}, u32[]{:S(2)}, u32[]{:S(2)}) %collective-permute-start) | collective-permute-done | bytes 61472 | tf_op jit(solution)/shard_map/ppermute | solution.py:23
  30.3 0.8 fusion.30
  31.1 1.1 fusion.31
  32.2 0.2 stack.127
  32.4 2.5 %collective-permute-start.1 = (f32[31,1024]{1,0:T(8,128)S(1)}, f32[31,1024]{1,0:T(8,128)S(1)}, u32[]{:S(2)}, u32[]{:S(2)}) collective-permute-start(f32[31,1024]{1,0:T(8,128)S(1)} %stack.127), channel_id=1, source_target_pairs={{0,2},{2,0},{4,6},{6,4},{8,10},{10,8},{12,14},{14,12},{16,18},{18,... | collective-permute-start | bytes 380936 | tf_op jit(solution)/shard_map/ppermute | solution.py:14
  34.9 4.6 %collective-permute-done.1 = f32[31,1024]{1,0:T(8,128)S(1)} collective-permute-done((f32[31,1024]{1,0:T(8,128)S(1)}, f32[31,1024]{1,0:T(8,128)S(1)}, u32[]{:S(2)}, u32[]{:S(2)}) %collective-permute-start.1) | collective-permute-done | bytes 127008 | tf_op jit(solution)/shard_map/ppermute | solution.py:14
  39.5 2.8 %collective-permute-start.2 = (f32[31,1024]{1,0:T(8,128)S(1)}, f32[31,1024]{1,0:T(8,128)S(1)}, u32[]{:S(2)}, u32[]{:S(2)}) collective-permute-start(f32[31,1024]{1,0:T(8,128)S(1)} %add.48), channel_id=1, source_target_pairs={{0,4},{2,6},{4,0},{6,2},{8,12},{10,14},{12,8},{14,10},{16,20},{18,... | collective-permute-start | bytes 380936 | tf_op jit(solution)/shard_map/ppermute | solution.py:14
  42.4 3.3 %collective-permute-done.2 = f32[31,1024]{1,0:T(8,128)S(1)} collective-permute-done((f32[31,1024]{1,0:T(8,128)S(1)}, f32[31,1024]{1,0:T(8,128)S(1)}, u32[]{:S(2)}, u32[]{:S(2)}) %collective-permute-start.2) | collective-permute-done | bytes 127008 | tf_op jit(solution)/shard_map/ppermute | solution.py:14
  45.7 3.3 %collective-permute-start.3 = (f32[31,1024]{1,0:T(8,128)S(1)}, f32[31,1024]{1,0:T(8,128)S(1)}, u32[]{:S(2)}, u32[]{:S(2)}) collective-permute-start(f32[31,1024]{1,0:T(8,128)S(1)} %add.49), channel_id=1, source_target_pairs={{0,8},{2,10},{4,12},{6,14},{8,0},{10,2},{12,4},{14,6},{16,24},{18,... | collective-permute-start | bytes 380936 | tf_op jit(solution)/shard_map/ppermute | solution.py:14
  49.1 3.3 %collective-permute-done.3 = f32[31,1024]{1,0:T(8,128)S(1)} collective-permute-done((f32[31,1024]{1,0:T(8,128)S(1)}, f32[31,1024]{1,0:T(8,128)S(1)}, u32[]{:S(2)}, u32[]{:S(2)}) %collective-permute-start.3) | collective-permute-done | bytes 127008 | tf_op jit(solution)/shard_map/ppermute | solution.py:14
  52.4 3.8 %collective-permute-start.4 = (f32[31,1024]{1,0:T(8,128)S(1)}, f32[31,1024]{1,0:T(8,128)S(1)}, u32[]{:S(2)}, u32[]{:S(2)}) collective-permute-start(f32[31,1024]{1,0:T(8,128)S(1)} %add.50), channel_id=1, source_target_pairs={{0,16},{2,18},{4,20},{6,22},{8,24},{10,26},{12,28},{14,30},{16,0},... | collective-permute-start | bytes 380936 | tf_op jit(solution)/shard_map/ppermute | solution.py:14
  56.2 0.1 copy.24
  56.3 0.1 copy.23
  56.4 4.4 %collective-permute-done.4 = f32[31,1024]{1,0:T(8,128)S(1)} collective-permute-done((f32[31,1024]{1,0:T(8,128)S(1)}, f32[31,1024]{1,0:T(8,128)S(1)}, u32[]{:S(2)}, u32[]{:S(2)}) %collective-permute-start.4) | collective-permute-done | bytes 127008 | tf_op jit(solution)/shard_map/ppermute | solution.py:14
  60.8 0.8 multiply_subtract_fusion.1
  61.6 42.4 %reduce-scatter.5.cloned.1.call-done = f32[128,128]{0,1:T(8,128)} async-done(((f32[2048,128]{0,1:T(8,128)}), f32[128,128]{0,1:T(8,128)}) %reduce-scatter.5.cloned.1.call-update) | async-done | bytes 65552 | tf_op jit(solution)/shard_map/reduce_scatter | solution.py:54
  104.0 0.9 rsqrt_multiply_fusion
  104.9 1.9 %all_gather.3 = f32[128,256]{0,1:T(8,128)S(1)} all-gather(f32[128,128]{0,1:T(8,128)S(1)} %get-tuple-element.61), channel_id=1, replica_groups=mesh['fs'=16,'tp'=2] {'tp'}, dimensions={1}, use_global_device_ids=true | all-gather | bytes 196608 | tf_op jit(solution)/shard_map/all_gather | solution.py:58
  106.8 1.1 multiply_reduce_fusion
  107.9 2.5 %psum.7 = f32[128]{0:T(128)S(1)} all-reduce(f32[128]{0:T(128)S(1)} %get-tuple-element.64), channel_id=1, replica_groups=mesh['fs'=16,'tp'=2] {'tp'}, use_global_device_ids=true, to_apply=%region_3.0 | all-reduce | flops 128 | bytes 1024 | tf_op jit(solution)/shard_map/psum | solution.py:60
  110.4 0.7 copy.25
  111.1 0.7 copy.26
  111.8 1.8 %fusion.37 = (bf16[128,2048]{1,0:T(8,128)(2,1)}, f32[128,2048]{1,0:T(8,128)}, f32[128,2048]{1,0:T(8,128)}) fusion(f32[128,2048]{1,0:T(8,128)S(1)} %copy-done.2, f32[128,2048]{1,0:T(8,128)S(1)} %get-tuple-element.65, f32[128]{0:T(128)S(1)} %add_sqrt_fusion), kind=kLoop, calls=%fused_computation.81 | loop fusion | flops 1048576 | bytes 4719104 | tf_op jit(solution)/shard_map/convert_element_type | solution.py:63
  (30 shorter events, 0.3 us)
Async XLA Ops:
  7.2 1.2 %copy-start = (bf16[2048,256]{1,0:T(8,128)(2,1)S(1)}, bf16[2048,256]{1,0:T(8,128)(2,1)}, u32[]{:S(2)}) copy-start(bf16[2048,256]{1,0:T(8,128)(2,1)} %param.15) | copy-start | bytes 3145732
  7.2 13.9 %reduce-scatter.7.cloned.1.call-start = ((), (), s32[]{:S(2)}) async-start(), calls=%async_computation.3 | async-start | bytes 98304
  8.4 13.6 %copy-start.1 = (bf16[128,2048]{1,0:T(8,128)(2,1)S(1)}, bf16[128,2048]{1,0:T(8,128)(2,1)}, u32[]{:S(2)}) copy-start(bf16[128,2048]{1,0:T(8,128)(2,1)} %param.12) | copy-start | bytes 1572868
  10.6 93.5 %reduce-scatter.5.cloned.1.call-start = ((), (), s32[]{:S(2)}) async-start(), calls=%async_computation.2 | async-start | bytes 1114112 | tf_op jit(solution)/shard_map/reduce_scatter | solution.py:54
  21.0 1.0 copy-start.5
  23.6 0.9 copy-start.4
  24.6 5.7 %copy-start.3 = (bf16[128,1024]{1,0:T(8,128)(2,1)S(1)}, bf16[128,1024]{1,0:T(8,128)(2,1)}, u32[]{:S(2)}) copy-start(bf16[128,1024]{1,0:T(8,128)(2,1)} %param.14) | copy-start | bytes 786436
  24.6 5.6 %collective-permute-start = (bf16[30,1024]{1,0:T(8,128)(2,1)S(1)}, bf16[30,1024]{1,0:T(8,128)(2,1)S(1)}, u32[]{:S(2)}, u32[]{:S(2)}) collective-permute-start(bf16[30,1024]{1,0:T(8,128)(2,1)S(1)} %slice.96), channel_id=1, source_target_pairs={{0,2},{2,4},{4,6},{6,8},{8,10},{10,12},{12,14},{14,16},{16,18},{18... | collective-permute-start | bytes 184328 | tf_op jit(solution)/shard_map/ppermute | solution.py:23
  32.4 7.1 %collective-permute-start.1 = (f32[31,1024]{1,0:T(8,128)S(1)}, f32[31,1024]{1,0:T(8,128)S(1)}, u32[]{:S(2)}, u32[]{:S(2)}) collective-permute-start(f32[31,1024]{1,0:T(8,128)S(1)} %stack.127), channel_id=1, source_target_pairs={{0,2},{2,0},{4,6},{6,4},{8,10},{10,8},{12,14},{14,12},{16,18},{18,... | collective-permute-start | bytes 380936 | tf_op jit(solution)/shard_map/ppermute | solution.py:14
  39.5 6.1 %collective-permute-start.2 = (f32[31,1024]{1,0:T(8,128)S(1)}, f32[31,1024]{1,0:T(8,128)S(1)}, u32[]{:S(2)}, u32[]{:S(2)}) collective-permute-start(f32[31,1024]{1,0:T(8,128)S(1)} %add.48), channel_id=1, source_target_pairs={{0,4},{2,6},{4,0},{6,2},{8,12},{10,14},{12,8},{14,10},{16,20},{18,... | collective-permute-start | bytes 380936 | tf_op jit(solution)/shard_map/ppermute | solution.py:14
  45.7 10.5 %copy-start.9 = (f32[128,128]{1,0:T(8,128)S(1)}, f32[128,128]{1,0:T(8,128)}, u32[]{:S(2)}) copy-start(f32[128,128]{1,0:T(8,128)} %param.18) | copy-start | bytes 196612
  45.7 6.6 %collective-permute-start.3 = (f32[31,1024]{1,0:T(8,128)S(1)}, f32[31,1024]{1,0:T(8,128)S(1)}, u32[]{:S(2)}, u32[]{:S(2)}) collective-permute-start(f32[31,1024]{1,0:T(8,128)S(1)} %add.49), channel_id=1, source_target_pairs={{0,8},{2,10},{4,12},{6,14},{8,0},{10,2},{12,4},{14,6},{16,24},{18,... | collective-permute-start | bytes 380936 | tf_op jit(solution)/shard_map/ppermute | solution.py:14
  52.4 3.9 %copy-start.10 = (f32[128,128]{1,0:T(8,128)S(1)}, f32[128,128]{1,0:T(8,128)}, u32[]{:S(2)}) copy-start(f32[128,128]{1,0:T(8,128)} %param.17) | copy-start | bytes 196612
  52.4 8.4 %copy-start.8 = (f32[31,1024]{1,0:T(8,128)S(1)}, f32[31,1024]{1,0:T(8,128)}, u32[]{:S(2)}) copy-start(f32[31,1024]{1,0:T(8,128)} %param.21) | copy-start | bytes 380932
  52.4 8.4 %copy-start.6 = (f32[31,1024]{1,0:T(8,128)S(1)}, f32[31,1024]{1,0:T(8,128)}, u32[]{:S(2)}) copy-start(f32[31,1024]{1,0:T(8,128)} %param.19) | copy-start | bytes 380932
  52.4 8.4 %copy-start.7 = (f32[31,1024]{1,0:T(8,128)S(1)}, f32[31,1024]{1,0:T(8,128)}, u32[]{:S(2)}) copy-start(f32[31,1024]{1,0:T(8,128)} %param.20) | copy-start | bytes 380932
  52.4 8.4 %collective-permute-start.4 = (f32[31,1024]{1,0:T(8,128)S(1)}, f32[31,1024]{1,0:T(8,128)S(1)}, u32[]{:S(2)}, u32[]{:S(2)}) collective-permute-start(f32[31,1024]{1,0:T(8,128)S(1)} %add.50), channel_id=1, source_target_pairs={{0,16},{2,18},{4,20},{6,22},{8,24},{10,26},{12,28},{14,30},{16,0},... | collective-permute-start | bytes 380936 | tf_op jit(solution)/shard_map/ppermute | solution.py:14
  106.8 5.0 %copy-start.2 = (f32[128,2048]{1,0:T(8,128)S(1)}, f32[128,2048]{1,0:T(8,128)}, u32[]{:S(2)}) copy-start(f32[128,2048]{1,0:T(8,128)} %param.16) | copy-start | bytes 3145732
Sparse Core Ops, SparseCore 0:
  10.8 10.2 reduce-scatter.6
  23.9 80.1 reduce-scatter.4
